TPU v7x, 512 devices: a whole 4x4x16 slice. The times are simulated.
512 devices in a mesh: gr: 2 (over z_hi), fs: 32 (over z_lo, y), tp: 8 (over x, core).
Axes of the slice: x: 4, y: 4, z: 16 (z_hi: 2, z_lo: 8; z = z_hi * 8 + z_lo), core: 2. Of those that a mesh axis runs over, the one named last changes fastest.
Arguments:
- tokens: bfloat16 [12288, 2048], P(('gr', 'fs')), may hold values from -6 to 6
- routes: int32 [12288, 8], P(('gr', 'fs')), may hold values from 0 to 63, all different within a row; in each aligned block of 192 rows (0 to 191, 192 to 383, ...) at most 36 rows name the same one
- route_weight: float32 [12288, 8], P(('gr', 'fs')), may hold values from 0.05 to 0.6
- norm_gain: float32 [2048], replicated, may hold values from 0.1 to 1.9
- gate_experts: float32 [2, 32, 512, 2048], P('gr', None, 'fs', 'tp'), may hold values from -0.125 to 0.125
- up_experts: float32 [2, 32, 512, 2048], P('gr', None, 'fs', 'tp'), may hold values from -0.125 to 0.125
- down_experts: float32 [2, 32, 512, 2048], P('gr', None, 'fs', 'tp'), may hold values from -0.25 to 0.25
- gate_shared: float32 [2048, 512], P('fs', 'tp'), may hold values from -0.125 to 0.125
- up_shared: float32 [2048, 512], P('fs', 'tp'), may hold values from -0.125 to 0.125
- down_shared: float32 [512, 2048], P('fs', 'tp'), may hold values from -0.25 to 0.25
Outputs:
- mixed: bfloat16 [12288, 2048], P(('gr', 'fs'), 'tp')
- gate_served: bfloat16 [2, 32, 512, 2048], P(None, 'fs', 'tp')
- up_served: bfloat16 [2, 32, 512, 2048], P(None, 'fs', 'tp')
- down_served: bfloat16 [2, 32, 512, 2048], P(None, 'fs', None, 'tp')
- gate_shared_served: bfloat16 [2048, 512], P(None, 'tp')
- up_shared_served: bfloat16 [2048, 512], P(None, 'tp')
- down_shared_served: bfloat16 [512, 2048], P(None, 'tp')
Inputs may be any that keep to these rules, and one draw needn't show every extreme that they name: `routes`: each row names 8 different experts; within the 192 rows of one device no expert is named by more than 36 rows, and some expert reaches 36.
All inputs are finite; a program needn't handle non-finite values.
Results may differ from a plain program's by a relative error of at most 0.0084.
Values may be sent and summed in bfloat16 or wider, within the bound.
No kernel may reach another device: no remote copies, remote signals or barrier semaphores. Data moves between devices by JAX's collectives and lax.ppermute only.
A program may use at most 128 MiB of HBM per device.

v0:
```python
import jax
import jax.numpy as jnp
from jax import lax
from jax.sharding import PartitionSpec as P

EXP_HALF = 1


EPS = 1e-06


def sent_to_all(shard, axis):
    copies = jnp.broadcast_to(shard, (lax.axis_size(axis), *shard.shape))
    return lax.all_to_all(copies, axis, split_axis=0, concat_axis=0, tiled=True)


def joined_along(parts, dim):
    dims = list(parts.shape[1:])
    dims[dim] *= parts.shape[0]
    return jnp.moveaxis(parts, 0, dim).reshape(dims)


def collect(shard, axis, dim):
    parts = sent_to_all(shard, axis)
    return joined_along(parts, dim)


def side_by_side(arrays, axis, dim, along):
    widths = [a.shape[along] for a in arrays]
    both = jnp.concatenate(arrays, axis=along)
    whole = collect(both, axis, dim)
    return tuple(jnp.split(whole, [sum(widths[:k]) for k in range(1, len(widths))], axis=along))


def sent_together(arrays, axis, split_dim, concat_dim, along):
    widths = [a.shape[along] for a in arrays]
    both = jnp.concatenate(arrays, axis=along)
    whole = lax.all_to_all(both, axis, split_axis=split_dim, concat_axis=concat_dim, tiled=True)
    return tuple(jnp.split(whole, [sum(widths[:k]) for k in range(1, len(widths))], axis=along))


def in_one_piece(arrays, axis, dim, along):
    both = jnp.concatenate(arrays, axis=along)
    whole, at, gathered = (lax.all_gather(both, axis, axis=dim, tiled=True), 0, [])
    for a in arrays:
        gathered.append(lax.slice_in_dim(whole, at, at + a.shape[along], axis=along))
        at += a.shape[along]
    return tuple(gathered)


def on_device(
    tokens,
    routes,
    route_weight,
    norm_gain,
    gate_experts,
    up_experts,
    down_experts,
    gate_shared,
    up_shared,
    down_shared,
):
    bf = jnp.bfloat16
    f32 = jnp.float32
    n_fs = lax.axis_size("fs")
    n_gr = lax.axis_size("gr")
    n_tp = lax.axis_size("tp")
    fs_index = lax.axis_index("fs")
    cols_here = gate_experts.shape[3]
    gain_cols = lax.dynamic_slice_in_dim(norm_gain, lax.axis_index("tp") * cols_here, cols_here, 0)
    gate_local = (gate_experts * gain_cols[None, None, None, :]).astype(bf)
    up_local = (up_experts * gain_cols[None, None, None, :]).astype(bf)
    down_local = down_experts.astype(bf)
    shared_here = gate_shared.shape[0]
    gain_shared = lax.dynamic_slice_in_dim(norm_gain, fs_index * shared_here, shared_here, 0)
    gate_sh_local = (gate_shared * gain_shared[:, None]).astype(bf)
    up_sh_local = (up_shared * gain_shared[:, None]).astype(bf)
    down_sh_local = down_shared.astype(bf)
    halves = side_by_side((gate_local, up_local, down_local), "gr", 0, 1)
    gate_cols, up_cols, down_w = sent_together((halves[0], halves[1], halves[2]), "fs", 1, 2, 0)
    gate_w, up_w = sent_together((gate_cols, up_cols), "tp", 2, 3, 0)
    gate_sw, up_sw, down_sw = (
        *in_one_piece((gate_sh_local, up_sh_local), "fs", 0, 1),
        lax.all_gather(down_sh_local, "fs", axis=0, tiled=True),
    )
    values = tokens.astype(f32)
    normed = (values * lax.rsqrt(jnp.mean(values * values, axis=-1, keepdims=True) + EPS)).astype(
        bf
    )
    tok_count, top = routes.shape
    width = tokens.shape[1]
    per_group = gate_experts.shape[1]
    count = per_group * n_gr
    capacity = (3 * tok_count * top + 2 * count - 1) // (2 * count)
    flat_e = routes.reshape(-1)
    onehot = (flat_e[:, None] == jnp.arange(count, dtype=jnp.int32)[None, :]).astype(jnp.int32)
    ranks = jnp.sum(jnp.cumsum(onehot, axis=0) * onehot, axis=1) - 1
    group_of = flat_e // per_group
    within = flat_e % per_group
    target = within // EXP_HALF
    local_k = within % EXP_HALF
    slot = ((target * n_gr + group_of) * EXP_HALF + local_k) * capacity + ranks
    total_slots = n_fs * n_gr * EXP_HALF * capacity
    repeated = jnp.repeat(normed, top, axis=0)
    send = jnp.zeros((total_slots, width), bf).at[slot].set(repeated)
    send = send.reshape(n_fs, n_gr, EXP_HALF, capacity, width)
    cols = width // n_tp
    send = lax.dynamic_slice_in_dim(send, lax.axis_index("tp") * cols, cols, 4)
    received = lax.all_to_all(send, "fs", split_axis=0, concat_axis=0, tiled=True)
    received = lax.all_gather(received, "tp", axis=4, tiled=True)
    gate = jnp.einsum("sgkcd,gkfd->sgkcf", received, gate_w, preferred_element_type=f32)
    upper = jnp.einsum("sgkcd,gkfd->sgkcf", received, up_w, preferred_element_type=f32)
    hidden = (jax.nn.silu(gate) * upper).astype(bf)
    full_hidden = collect(hidden, "tp", 4)
    result = jnp.einsum(
        "sgkcf,gkfe->sgkce", full_hidden, down_w, preferred_element_type=f32
    ).astype(bf)
    returned = lax.all_to_all(result, "fs", split_axis=0, concat_axis=0, tiled=True)
    picked = returned.reshape(total_slots, cols)[slot].reshape(tok_count, top, cols)
    routed = jnp.einsum("tkc,tk->tc", picked.astype(f32), route_weight)
    shared_gate = jnp.dot(normed, gate_sw, preferred_element_type=f32)
    shared_up = jnp.dot(normed, up_sw, preferred_element_type=f32)
    shared_hidden = (jax.nn.silu(shared_gate) * shared_up).astype(bf)
    shared_full = collect(shared_hidden, "tp", 1)
    shared = jnp.dot(shared_full, down_sw, preferred_element_type=f32)
    mixed = (routed + shared).astype(bf)
    return (mixed, gate_w, up_w, down_w, gate_sw, up_sw, down_sw)


def solution(mesh):
    return jax.shard_map(
        on_device,
        mesh=mesh,
        in_specs=(
            P(("gr", "fs"), None),
            P(("gr", "fs"), None),
            P(("gr", "fs"), None),
            P(),
            P("gr", None, "fs", "tp"),
            P("gr", None, "fs", "tp"),
            P("gr", None, "fs", "tp"),
            P("fs", "tp"),
            P("fs", "tp"),
            P("fs", "tp"),
        ),
        out_specs=(
            P(("gr", "fs"), "tp"),
            P(None, "fs", "tp", None),
            P(None, "fs", "tp", None),
            P(None, "fs", None, "tp"),
            P(None, "tp"),
            P(None, "tp"),
            P(None, "tp"),
        ),
        check_vma=False,
    )
```

profile of v0, /device:TPU:1, one launch (start us, length us, event | category | flops | bytes accessed | tf_op | source)
XLA Modules:
  0.0 694.6 jit_solution(2489082165161462181)
XLA Ops:
  7.2 0.9 copy.80
  8.4 1.4 fusion.8
  9.8 0.2 fusion.9
  10.1 18.1 %reduce-window.6 = s32[64,12,128]{2,1,0:T(8,128)S(1)} reduce-window(s32[64,12,128]{2,1,0:T(8,128)S(1)} %fusion.32, s32[]{:T(128)} %constant.70.clone.1), window={size=1x1x128 pad=0_0x0_0x127_0}, to_apply=%region_0.0 | reduce-window | flops 12484608 | bytes 786436 | tf_op jit(solution)/shard_map/reduce-window
  28.2 0.2 slice.24
  28.4 0.3 copy.83
  28.8 0.2 broadcast_add_fusion
  29.0 0.1 fusion.34
  29.3 14.6 %scatter_custom_fusion = bf16[2304,2048]{1,0:T(8,128)(2,1)} fusion(s32[1536]{0:T(1024)S(1)} %fusion.35, bf16[]{:T(256)} %constant.72.clone.1, bf16[192,2048]{1,0:T(8,128)(2,1)S(1)} %fusion.9), kind=kCustom, calls=%fused_computation.6 | custom fusion | bytes 10223618 | tf_op jit(solution)/shard_map/scatter | solution.py:105
  43.9 13.1 %reshape.234 = bf16[32,2,1,36,2048]{4,3,1,0,2:T(8,128)(2,1)} reshape(bf16[2304,2048]{1,0:T(8,128)(2,1)} %scatter_custom_fusion) | data formatting | bytes 18874368 | tf_op jit(solution)/shard_map/reshape | solution.py:106
  57.0 1.4 constant_dynamic-slice_fusion
  58.4 0.9 copy.85
  59.3 73.5 %all_to_all.49 = bf16[32,2,1,36,256]{4,1,3,2,0:T(2,128)(2,1)S(1)} all-to-all(bf16[32,2,1,36,256]{4,1,3,2,0:T(2,128)(2,1)S(1)} %copy.85), channel_id=1, replica_groups=mesh['gr'=2,'fs'=32,'tp'=8] {'fs'}, dimensions={0} | all-to-all | bytes 2359296 | tf_op jit(solution)/shard_map/all_to_all | solution.py:109
  132.8 1.3 copy.86
  134.1 0.8 dynamic_slice.9
  135.0 0.1 copy-done.6
  135.1 0.2 copy-done.7
  135.3 0.1 multiply_convert_fusion.1
  135.6 42.3 %all_to_all.50 = bf16[2,1,96,16,256]{4,3,2,1,0:T(8,128)(2,1)S(1)} all-to-all(bf16[2,1,96,16,256]{4,3,2,1,0:T(8,128)(2,1)S(1)} %broadcast_in_dim.10), channel_id=1, replica_groups=mesh['gr'=2,'fs'=32,'tp'=8] {'gr'}, dimensions={0} | all-to-all | bytes 3145728 | tf_op jit(solution)/shard_map/all_to_all | solution.py:14
  178.0 0.2 pad_maximum_fusion
  178.2 0.2 copy.73
  178.3 122.1 %all_to_all.51 = bf16[6,32,16,256]{3,2,0,1:T(8,128)(2,1)S(1)} all-to-all(bf16[6,32,16,256]{3,2,0,1:T(8,128)(2,1)S(1)} %copy.73), channel_id=1, replica_groups=mesh['gr'=2,'fs'=32,'tp'=8] {'fs'}, dimensions={1} | all-to-all | bytes 3145728 | tf_op jit(solution)/shard_map/all_to_all | solution.py:38
  300.8 0.8 copy.77
  301.6 21.3 %all_to_all.52 = bf16[4,1,512,256]{3,0,1,2:T(4,128)(2,1)S(1)} all-to-all(bf16[4,1,512,256]{3,0,1,2:T(4,128)(2,1)S(1)} %copy.77), channel_id=1, replica_groups=mesh['gr'=2,'fs'=32,'tp'=8] {'tp'}, dimensions={2} | all-to-all | bytes 2097152 | tf_op jit(solution)/shard_map/all_to_all | solution.py:38
  322.9 0.1 copy.78
  323.0 1.0 slice_bitcast_fusion
  324.0 0.3 copy.79
  324.3 1.0 reshape.257
  325.4 0.3 copy.87
  325.7 1.0 reshape.258
  326.7 5.9 fusion.11
  332.6 1.5 copy-done.12
  334.0 3.2 fusion.23
  337.4 3.0 broadcast_bitcast_fusion
  340.4 7.9 %reshape.268 = bf16[8,2,73728]{2,1,0:T(2,128)(2,1)} reshape(bf16[8,1,2,36,32,64]{5,4,3,2,1,0:T(8,128)(2,1)} %broadcast_bitcast_fusion) | data formatting | bytes 4718592
  348.3 5.3 all-to-all-start.4
  353.7 29.1 %all-to-all-done.4 = bf16[8,2,73728]{2,1,0:T(2,128)(2,1)} async-done(((bf16[8,2,73728]{2,1,0:T(2,128)(2,1)}), bf16[8,2,73728]{2,1,0:T(2,128)(2,1)}, u32[]{:S(2)}, u32[]{:S(2)}) %all-to-all-start.4) | async-done | bytes 2359328 | tf_op jit(solution)/shard_map/all_to_all | solution.py:14
  382.8 7.7 %reshape.269 = bf16[8,1,2,36,32,64]{5,4,3,2,1,0:T(8,128)(2,1)} reshape(bf16[8,2,73728]{2,1,0:T(2,128)(2,1)} %all-to-all-done.4) | data formatting | bytes 4718592
  390.5 3.1 bitcast_bitcast_fusion.1
  393.6 5.2 copy.105
  398.8 7.3 %reshape.264 = bf16[32,2,36,512]{3,2,0,1:T(8,128)(2,1)} reshape(bf16[32,2,1,36,8,64]{5,4,3,0,1,2:T(8,128)(2,1)} %copy.105) | data formatting | bytes 4718592 | tf_op jit(solution)/shard_map/reshape.37
  406.1 2.6 fusion.10
  408.7 2.2 copy.91
  410.9 5.6 all-to-all-start.5
  416.6 0.8 dynamic_slice.11
  417.3 0.1 copy.103
  417.7 120.1 %all_gather.10 = bf16[2048,128]{1,0:T(8,128)(2,1)S(1)} all-gather(bf16[64,128]{1,0:T(8,128)(2,1)S(1)} %pad_maximum_fusion.2), channel_id=1, replica_groups=mesh['gr'=2,'fs'=32,'tp'=8] {'fs'}, dimensions={0}, use_global_device_ids=true | all-gather | bytes 540672 | tf_op jit(solution)/shard_map/all_gather | solution.py:44
  537.8 1.1 fusion.43
  538.9 1.9 copy.98
  540.8 1.9 copy.99
  542.8 100.0 %all_gather.11 = bf16[512,256]{1,0:T(8,128)(2,1)S(1)} all-gather(bf16[16,256]{1,0:T(8,128)(2,1)S(1)} %convert_element_type.64), channel_id=1, replica_groups=mesh['gr'=2,'fs'=32,'tp'=8] {'fs'}, dimensions={0}, use_global_device_ids=true | all-gather | bytes 270336 | tf_op jit(solution)/shard_map/all_gather | solution.py:84
  642.8 0.4 fusion.39
  643.2 0.7 fusion.27
  643.9 0.8 copy.110
  644.8 0.8 copy.111
  645.6 0.8 broadcast_in_dim.27
  646.4 0.4 copy-done
  646.8 32.6 %all-to-all-start.6 = ((bf16[8,192,64]{1,2,0:T(8,128)(2,1)}), bf16[8,192,64]{1,2,0:T(8,128)(2,1)S(1)}, u32[]{:S(2)}, u32[]{:S(2)}) async-start(bf16[8,192,64]{1,2,0:T(8,128)(2,1)} %broadcast_in_dim.27), calls=%async_computation.6 | async-start | bytes 524288 | tf_op jit(solution)/shard_map/all_to_all | solution.py:14
  679.3 1.5 copy.92
  680.8 0.3 reshape.238
  681.1 4.8 gather_fusion
  685.8 0.4 fusion.28
  686.2 0.9 fusion.26
  687.1 0.7 copy.116
  (50 shorter events, 1.6 us)
Async XLA Ops:
  7.2 2.6 copy-start.1
  7.2 319.5 %all-gather.2.cloned.1.call-start = ((), (), s32[]{:S(2)}) async-start(), calls=%async_computation.7 | async-start | bytes 11796480 | tf_op jit(solution)/shard_map/all_gather | solution.py:110
  132.8 1.3 copy-start.3
  134.0 1.0 copy-start.6
  134.0 1.2 copy-start.7
  326.7 5.9 copy-start.5
  326.7 7.3 %copy-start.12 = (bf16[32,2,1,36,2048]{4,3,0,1,2:T(8,128)(2,1)S(1)}, bf16[32,2,1,36,2048]{4,3,0,1,2:T(8,128)(2,1)}, u32[]{:S(2)}) copy-start(bf16[32,2,1,36,2048]{4,3,0,1,2:T(8,128)(2,1)} %all-gather.2.cloned.1.call-done) | copy-start | bytes 28311556
  348.3 34.4 %all-to-all-start.4 = ((bf16[8,2,73728]{2,1,0:T(2,128)(2,1)}), bf16[8,2,73728]{2,1,0:T(2,128)(2,1)}, u32[]{:S(2)}, u32[]{:S(2)}) async-start(bf16[8,2,73728]{2,1,0:T(2,128)(2,1)} %reshape.268), calls=%async_computation.4 | async-start | bytes 4718592 | tf_op jit(solution)/shard_map/all_to_all | solution.py:14
  353.7 52.5 %copy-start.4 = (bf16[2,32,16,256]{3,2,1,0:T(8,128)(2,1)}, bf16[2,32,16,256]{3,2,1,0:T(8,128)(2,1)S(1)}, u32[]{:S(2)}) copy-start(bf16[2,32,16,256]{3,2,1,0:T(8,128)(2,1)S(1)} %copy.107) | copy-start | bytes 1572868
  410.9 6.4 copy-start.10
  410.9 6.4 copy-start.11
  410.9 6.6 copy-start.8
  410.9 6.6 copy-start.9
  410.9 234.7 %all-to-all-start.5 = ((bf16[32,2,1,36,256]{4,1,3,2,0:T(2,128)(2,1)}), bf16[32,2,1,36,256]{4,1,3,2,0:T(2,128)(2,1)S(1)}, u32[]{:S(2)}, u32[]{:S(2)}) async-start(bf16[32,2,1,36,256]{4,1,3,2,0:T(2,128)(2,1)} %copy.91), calls=%async_computation.5 | async-start | bytes 2359296 | tf_op jit(solution)/shard_map/all_to_all | solution.py:118
  542.8 101.1 %copy-start.2 = (bf16[1,2,8,8,8,256]{5,4,3,2,1,0:T(8,128)(2,1)S(1)}, bf16[1,2,8,8,8,256]{5,4,3,2,1,0:T(8,128)(2,1)}, u32[]{:S(2)}) copy-start(bf16[1,2,8,8,8,256]{5,4,3,2,1,0:T(8,128)(2,1)} %get-tuple-element.35) | copy-start | bytes 1572868
  645.6 1.1 copy-start
  646.8 39.4 %all-to-all-start.6 = ((bf16[8,192,64]{1,2,0:T(8,128)(2,1)}), bf16[8,192,64]{1,2,0:T(8,128)(2,1)S(1)}, u32[]{:S(2)}, u32[]{:S(2)}) async-start(bf16[8,192,64]{1,2,0:T(8,128)(2,1)} %broadcast_in_dim.27), calls=%async_computation.6 | async-start | bytes 524288 | tf_op jit(solution)/shard_map/all_to_all | solution.py:14
Sparse Core Ops, SparseCore 0:
  134.2 66.9 all-gather.1
where the time goes:
time: 696 us; the launch traced here: 695 us
  blocking collectives  479 us (69%)
  local copies, waits for them, and re-layouts  93.5 us (13%)
  starting transfers between devices  43.5 us (6%)
  waiting for transfers between devices  29.1 us (4%)
  other arithmetic  20.9 us (3%)
  between operations  14.4 us (2%)
  matrix products  14 us (2%)
    all_to_all x2, blocking collectives, sent_together(): lax.all_to_all(both, axis, split_axis=split_dim, concat_axis=concat_dim,...  143 us
    all_gather x1, blocking collectives, in_one_piece(): lax.all_gather(both, axis, axis=dim, tiled=True)  120 us
    all_gather x1, blocking collectives, on_device(): lax.all_gather(down_sh_local, 'fs', axis=0, tiled=True)  100 us
    all_to_all x1, blocking collectives, on_device(): lax.all_to_all(send, 'fs', split_axis=0, concat_axis=0, tiled=True)  73.5 us
    all_to_all x1, blocking collectives, sent_to_all(): return lax.all_to_all(copies, axis, split_axis=0, concat_axis=0, tiled=True)  42.3 us
    all_to_all x2, starting transfers between devices, sent_to_all(): return lax.all_to_all(copies, axis, split_axis=0, concat_axis=0, tiled=True)  37.9 us
    all_to_all x2, waiting for transfers between devices, sent_to_all(): return lax.all_to_all(copies, axis, split_axis=0, concat_axis=0, tiled=True)  29.1 us
    unnamed x38, local copies, waits for them, and re-layouts  27.5 us
  transfers between devices with their start and end apart: 4, of which 1 were waited for; matrix products, arithmetic and copies ran while one was open for 3% of the time, Pallas kernels for 0%

commit v1 on v0

v1 whole, which is shorter than its diff:
```python
import functools

import jax
import jax.numpy as jnp
from jax import lax
from jax.experimental import pallas as pl
from jax.experimental.pallas import tpu as pltpu
from jax.sharding import Mesh, PartitionSpec as P

EPS = 1e-06
bf = jnp.bfloat16
f32 = jnp.float32
FS = ("zl", "y")
TP = ("x", "core")
GF = ("gr", "zl", "y")


def slot_match(rows, experts, cap, n_fs, first, rows_dim):
    shape = (rows, experts) if rows_dim == 0 else (experts, rows)
    r = lax.broadcasted_iota(jnp.int32, shape, rows_dim) + first
    e = lax.broadcasted_iota(jnp.int32, shape, 1 - rows_dim)
    groups = experts // n_fs
    base = cap * (groups * lax.rem(e, n_fs) + lax.div(e, n_fs))
    inside = (r >= base) & (r < base + cap)
    return jnp.where(inside, 1.0, 0.0).astype(bf)


def slot_number(shape, dim, cap, first):
    r = lax.broadcasted_iota(jnp.int32, shape, dim) + first
    return lax.rem(r, cap).astype(f32)


def pack_kernel(cap, n_fs, experts, cols, chunk, at_ref, tok_ref, route_ref, weight_ref,
                normed_ref, rank_ref, mix_ref, send_ref):
    values = tok_ref[...].astype(f32)
    scale = lax.rsqrt(jnp.mean(values * values, axis=-1, keepdims=True) + EPS)
    normed_ref[...] = (values * scale).astype(bf)
    count, top = route_ref.shape
    e = lax.broadcasted_iota(jnp.int32, (count, experts), 1)
    chosen = jnp.zeros((count, experts), f32)
    mix = jnp.zeros((count, experts), f32)
    for j in range(top):
        here = route_ref[:, j : j + 1] == e
        chosen = jnp.where(here, 1.0, chosen)
        mix = jnp.where(here, weight_ref[:, j : j + 1], mix)
    row = lax.broadcasted_iota(jnp.int32, (count, count), 0)
    col = lax.broadcasted_iota(jnp.int32, (count, count), 1)
    before = jnp.where(col < row, 1.0, 0.0).astype(bf)
    rank = jnp.dot(before, chosen.astype(bf), preferred_element_type=f32)
    rank = jnp.where(chosen > 0, rank, -1.0)
    rank_ref[...] = rank
    mix_ref[...] = mix
    rank = rank.astype(bf)
    mine = normed_ref[:, pl.ds(pl.multiple_of(at_ref[0] * cols, cols), cols)]
    total = send_ref.shape[0]
    for first in range(0, total, chunk):
        owner = slot_match(chunk, experts, cap, n_fs, first, 0)
        spread = lax.dot_general(owner, rank, (((1,), (1,)), ((), ())), preferred_element_type=f32)
        pick = spread == slot_number((chunk, count), 0, cap, first)
        pick = jnp.where(pick, 1.0, 0.0).astype(bf)
        send_ref[first : first + chunk, :] = jnp.dot(pick, mine, preferred_element_type=f32).astype(bf)


def hidden_kernel(cap, n_tp, n_gr, x_ref, gate_ref, up_ref, out_ref):
    units = gate_ref.shape[1]
    cols = x_ref.shape[2]
    rows = x_ref.shape[1]
    total = jnp.zeros((2 * n_gr * units, rows), f32)
    for p in range(n_tp):
        pieces = []
        for g in range(n_gr):
            pieces.append(gate_ref[g, :, p * cols : (p + 1) * cols])
            pieces.append(up_ref[g, :, p * cols : (p + 1) * cols])
        w = jnp.concatenate(pieces, axis=0)
        total += lax.dot_general(w, x_ref[p], (((1,), (1,)), ((), ())), preferred_element_type=f32)
    slot = lax.broadcasted_iota(jnp.int32, (units, rows), 1) + pl.program_id(0) * rows
    group = lax.rem(slot, cap * n_gr) // cap
    gate, up = total[:units], total[units : 2 * units]
    for g in range(1, n_gr):
        gate = jnp.where(group == g, total[2 * g * units : (2 * g + 1) * units], gate)
        up = jnp.where(group == g, total[(2 * g + 1) * units : (2 * g + 2) * units], up)
    out_ref[...] = (gate / (1.0 + jnp.exp(-gate)) * up).astype(bf)


def mix_kernel(cap, n_fs, experts, chunk, ret_ref, rank_ref, mix_ref, shared_ref, out_ref):
    rank = rank_ref[...].astype(bf)
    high = mix_ref[...].astype(bf)
    low = (mix_ref[...] - high.astype(f32)).astype(bf)
    count = rank.shape[0]
    total = shared_ref[...]
    for first in range(0, ret_ref.shape[0], chunk):
        owner = slot_match(chunk, experts, cap, n_fs, first, 1)
        spread = jnp.dot(rank, owner, preferred_element_type=f32)
        pick = spread == slot_number((count, chunk), 1, cap, first)
        part = ret_ref[first : first + chunk, :]
        for w in (high, low):
            weight = jnp.dot(w, owner, preferred_element_type=f32)
            weight = jnp.where(pick, weight, 0.0).astype(bf)
            total += jnp.dot(weight, part, preferred_element_type=f32)
    out_ref[...] = total.astype(bf)


def spread_to(block, axis):
    copies = jnp.broadcast_to(block[None], (lax.axis_size(axis), *block.shape))
    return lax.all_to_all(copies, axis, split_axis=0, concat_axis=0, tiled=True)


def silu(v):
    return v / (1.0 + jnp.exp(-v))


def on_device(tokens, routes, route_weight, norm_gain, gate_experts, up_experts, down_experts,
              gate_shared, up_shared, down_shared):
    n_gr, n_fs, n_tp = lax.axis_size("gr"), lax.axis_size(FS), lax.axis_size(TP)
    n_z, n_y = lax.axis_size("zl"), lax.axis_size("y")
    n_x = lax.axis_size("x")
    fs_at, tp_at, core = lax.axis_index(FS), lax.axis_index(TP), lax.axis_index("core")
    per_group, rows_here, cols = gate_experts.shape[1:]
    count, top = routes.shape
    width = tokens.shape[1]
    experts = per_group * n_gr
    cap = (3 * count * top + 2 * experts - 1) // (2 * experts)
    slots = experts * cap

    vmem = pltpu.CompilerParams(vmem_limit_bytes=48 * 1024 * 1024)
    normed, rank, mix, send = pl.pallas_call(
        functools.partial(pack_kernel, cap, n_fs, experts, cols, slots // 8),
        out_shape=(
            jax.ShapeDtypeStruct((count, width), bf),
            jax.ShapeDtypeStruct((count, experts), f32),
            jax.ShapeDtypeStruct((count, experts), f32),
            jax.ShapeDtypeStruct((slots, cols), bf),
        ),
        in_specs=[pl.BlockSpec(memory_space=pltpu.SMEM)] + [pl.BlockSpec(memory_space=pltpu.VMEM)] * 3,
        out_specs=(pl.BlockSpec(memory_space=pltpu.VMEM),) * 4,
        compiler_params=vmem,
        name="pack",
    )(tp_at.astype(jnp.int32).reshape(1), tokens, routes, route_weight)
    received = lax.all_to_all(send, FS, split_axis=0, concat_axis=0, tiled=True)
    rows_all = lax.all_gather(received, TP, axis=0, tiled=True).reshape(n_tp, slots, cols)

    gain = lax.dynamic_slice_in_dim(norm_gain, tp_at * cols, cols, 0)
    gate_local = (gate_experts[0] * gain).astype(bf)
    up_local = (up_experts[0] * gain).astype(bf)
    both = jnp.stack([gate_local, up_local], axis=1)
    both = jnp.broadcast_to(both[None], (n_gr, *both.shape)).reshape(n_gr * per_group, 2, rows_here, cols)
    both = lax.all_to_all(both, GF, split_axis=0, concat_axis=0, tiled=True)
    down_local = down_experts[0].astype(bf)
    down_all = jnp.broadcast_to(down_local[None], (n_gr, *down_local.shape)).reshape(-1, rows_here, cols)
    down_all = lax.all_to_all(down_all, GF, split_axis=0, concat_axis=0, tiled=True)
    down_w = down_all.reshape(n_gr, n_fs * rows_here, cols)

    near = n_fs // n_tp
    both = both.reshape(n_gr, n_tp, near, 2, rows_here, cols).transpose(1, 3, 0, 2, 4, 5)
    both = lax.all_to_all(both, TP, split_axis=0, concat_axis=0, tiled=True)
    units = near * rows_here
    both = both.reshape(n_tp, 2, n_gr, units, cols).transpose(1, 2, 3, 0, 4)
    gate_w, up_w = both[0].reshape(n_gr, units, width), both[1].reshape(n_gr, units, width)

    sh_rows, sh_cols = gate_shared.shape
    gain_sh = lax.dynamic_slice_in_dim(norm_gain, fs_at * sh_rows, sh_rows, 0)[:, None]
    pair = jnp.concatenate([(gate_shared * gain_sh).astype(bf), (up_shared * gain_sh).astype(bf)], axis=1)
    half = sh_rows * 2 * sh_cols // cols
    times = sh_rows // half
    pair = jnp.concatenate([pair[i * half : (i + 1) * half] for i in range(times)], axis=1)
    block = jnp.concatenate([pair, down_shared.astype(bf)], axis=0)
    block = spread_to(block, "zl")
    block = spread_to(block, "y")
    block = block.reshape(n_y, n_z, half + down_shared.shape[0], cols).transpose(1, 0, 2, 3)
    pair = block[:, :, :half].reshape(n_fs, half, times, 2 * sh_cols).transpose(0, 2, 1, 3)
    pair = pair.reshape(width, 2 * sh_cols)
    gate_sw, up_sw = pair[:, :sh_cols], pair[:, sh_cols:]
    down_sw = block[:, :, half:].reshape(-1, cols)

    turned = lax.dot_general(pair, normed, (((0,), (1,)), ((), ())), preferred_element_type=f32)
    shared_hidden = (silu(turned[:sh_cols]) * turned[sh_cols:]).astype(bf)

    row_block = slots // 6
    hidden = pl.pallas_call(
        functools.partial(hidden_kernel, cap, n_tp, n_gr),
        out_shape=jax.ShapeDtypeStruct((units, slots), bf),
        grid=(slots // row_block,),
        in_specs=[
            pl.BlockSpec((n_tp, row_block, cols), lambda i: (0, i, 0)),
            pl.BlockSpec((n_gr, units, width), lambda i: (0, 0, 0)),
            pl.BlockSpec((n_gr, units, width), lambda i: (0, 0, 0)),
        ],
        out_specs=pl.BlockSpec((units, row_block), lambda i: (0, i)),
        compiler_params=vmem,
        cost_estimate=pl.CostEstimate(
            flops=4 * n_gr * units * slots * width, bytes_accessed=2 * slots * width, transcendentals=units * slots
        ),
        name="gate_up",
    )(rows_all, gate_w, up_w)
    hidden = jnp.concatenate([hidden, shared_hidden], axis=1)
    near_hidden = spread_to(hidden, "x").reshape(n_x * units, slots + count)
    far_hidden = lax.ppermute(near_hidden, "core", [(0, 1), (1, 0)])

    def part(w, which):
        w = w.reshape(n_x, 2, units, *w.shape[1:])
        return lax.dynamic_index_in_dim(w, which, 1, keepdims=False).reshape(n_x * units, -1)

    def applied(lo, hi, w):
        turn = (((0,), (0,)), ((), ()))
        out = lax.dot_general(near_hidden[:, lo:hi], part(w, core), turn, preferred_element_type=f32)
        return out + lax.dot_general(far_hidden[:, lo:hi], part(w, 1 - core), turn, preferred_element_type=f32)

    down_cat = jnp.concatenate([down_w[g] for g in range(n_gr)], axis=1)
    result = applied(0, slots, down_cat)
    group = lax.rem(lax.broadcasted_iota(jnp.int32, (slots, cols), 0), cap * n_gr) // cap
    picked = result[:, :cols]
    for g in range(1, n_gr):
        picked = jnp.where(group == g, result[:, g * cols : (g + 1) * cols], picked)
    returned = lax.all_to_all(picked.astype(bf), FS, split_axis=0, concat_axis=0, tiled=True)
    shared = applied(slots, slots + count, down_sw)
    mixed = pl.pallas_call(
        functools.partial(mix_kernel, cap, n_fs, experts, slots // 6),
        out_shape=jax.ShapeDtypeStruct((count, cols), bf),
        in_specs=[pl.BlockSpec(memory_space=pltpu.VMEM)] * 4,
        out_specs=pl.BlockSpec(memory_space=pltpu.VMEM),
        compiler_params=vmem,
        name="mix",
    )(returned, rank, mix, shared)
    return (mixed, gate_w[:, None], up_w[:, None], down_w[:, None], gate_sw, up_sw, down_sw)


def solution(mesh):
    gr, fs, tp = mesh.devices.shape
    n_y = 4 if fs % 4 == 0 else 1
    fine = Mesh(mesh.devices.reshape(gr, fs // n_y, n_y, tp // 2, 2), ("gr", "zl", "y", "x", "core"))
    return jax.shard_map(
        on_device,
        mesh=fine,
        in_specs=(
            P(GF, None),
            P(GF, None),
            P(GF, None),
            P(),
            P("gr", None, FS, TP),
            P("gr", None, FS, TP),
            P("gr", None, FS, TP),
            P(FS, TP),
            P(FS, TP),
            P(FS, TP),
        ),
        out_specs=(
            P(GF, TP),
            P(None, FS, TP, None),
            P(None, FS, TP, None),
            P(None, FS, None, TP),
            P(None, TP),
            P(None, TP),
            P(None, TP),
        ),
        check_vma=False,
    )
```

time: 696 us -> 350 us (0.50)
  blocking collectives: 479 us -> 131 us
  waiting for transfers between devices: 29.1 us -> 113 us
  local copies, waits for them, and re-layouts: 93.5 us -> 26.6 us
  other arithmetic: 20.9 us -> 3.42 us
  Pallas kernels: 0 us -> 11.5 us
  matrix products: 14 us -> 4.5 us
    all_gather x2 -> x0, blocking collectives: 220 us -> none  [the longest x1 120 us: in_one_piece(): lax.all_gather(both, axis, axis=dim, tiled=True)]
    all_to_all x4 -> x2, blocking collectives: 259 us -> 131 us  [the longest x1 73.7 us: on_device(): received = lax.all_to_all(send, FS, split_axis=0, concat_axis=0, tiled=True)]
    all_to_all x3 -> x6, waiting for transfers between devices: 29.1 us -> 113 us  [the longest x1 43 us: on_device(): lax.all_to_all(picked.astype(bf), FS, split_axis=0, concat_axis=0, tiled=...]
    unnamed x38 -> x29, local copies, waits for them, and re-layouts: 27.5 us -> 8.04 us
    another operation x3 -> x1, other arithmetic: 18.4 us -> 0.05 us  [on_device(): both = jnp.stack([gate_local, up_local], axis=1)]
    scatter x1 -> x0, local copies, waits for them, and re-layouts: 14.6 us -> none  [on_device(): send = jnp.zeros((total_slots, width), bf).at[slot].set(repeated)]
    reshape x3 -> x2, local copies, waits for them, and re-layouts: 13.5 us -> 1.63 us  [the longest x1 1.5 us: on_device(): near_hidden = spread_to(hidden, 'x').reshape(n_x * units, slots + count)]
    pallas_call x0 -> x3, Pallas kernels: none -> 11.5 us  [the longest x1 7.46 us: on_device(): pl.pallas_call(functools.partial(hidden_kernel, cap, n_tp, n_gr), out_sha...]
  transfers between devices with their start and end apart: 4 -> 8, of which waited for: 1 -> 6; matrix products, arithmetic and copies ran while one was open for 3% -> 7% of each run, Pallas kernels for 0% -> 0%
where the time goes in v1:
time: 350 us; the launch traced here: 348 us
  blocking collectives  131 us (37%)
  waiting for transfers between devices  113 us (32%)
  starting transfers between devices  43.6 us (12%)
  local copies, waits for them, and re-layouts  26.6 us (8%)
  between operations  14.4 us (4%)
  Pallas kernels  11.5 us (3%)
  matrix products  4.5 us (1%)
    all_to_all x1, blocking collectives, on_device(): received = lax.all_to_all(send, FS, split_axis=0, concat_axis=0, tiled=True)  73.7 us
    all_to_all x1, blocking collectives, on_device(): both = lax.all_to_all(both, GF, split_axis=0, concat_axis=0, tiled=True)  57.5 us
    all_to_all x1, waiting for transfers between devices, on_device(): lax.all_to_all(picked.astype(bf), FS, split_axis=0, concat_axis=0, tiled=...  43 us
    all_to_all x3, waiting for transfers between devices, spread_to(): return lax.all_to_all(copies, axis, split_axis=0, concat_axis=0, tiled=True)  34.1 us
    all_to_all x1, waiting for transfers between devices, on_device(): lax.all_to_all(down_all, GF, split_axis=0, concat_axis=0, tiled=True)  23.7 us
    all_to_all x3, starting transfers between devices, spread_to(): return lax.all_to_all(copies, axis, split_axis=0, concat_axis=0, tiled=True)  16.8 us
    all_to_all x1, waiting for transfers between devices, on_device(): both = lax.all_to_all(both, TP, split_axis=0, concat_axis=0, tiled=True)  12.2 us
    all_to_all x1, starting transfers between devices, on_device(): both = lax.all_to_all(both, TP, split_axis=0, concat_axis=0, tiled=True)  9.9 us
  transfers between devices with their start and end apart: 8, of which 6 were waited for; matrix products, arithmetic and copies ran while one was open for 7% of the time, Pallas kernels for 0%

profile of v1, /device:TPU:1, one launch (start us, length us, event | category | flops | bytes accessed | tf_op | source)
XLA Modules:
  0.0 348.3 jit_solution(12927762684106238854)
XLA Ops:
  7.2 0.0 all-gather.2.cloned.1.call-start
  7.2 0.8 copy.74.route_ref
  8.0 0.8 copy.75.weight_ref
  8.9 1.1 copy-done
  10.0 1.6 pack.1
  11.7 73.7 %all_to_all.53 = bf16[32,72,256]{2,1,0:T(8,128)(2,1)} all-to-all(bf16[32,72,256]{2,1,0:T(8,128)(2,1)S(1)} %bitcast.58), channel_id=1, replica_groups=mesh['gr'=2,'zl'=8,'y'=4,'x'=4,'core'=2] {'zl','y'}, dimensions={0} | all-to-all | bytes 2359296 | tf_op jit(solution)/shard_map/all_to_all | solution.py:139
  85.4 0.0 all-gather.2.cloned.1.call-update
  85.4 0.8 dynamic_slice.21
  86.3 0.1 multiply_convert_fusion.1
  86.3 0.1 fusion.16
  86.4 0.1 fusion.13
  86.5 0.7 broadcast_in_dim.13
  87.2 5.2 %all-to-all-start.3 = ((bf16[8,48,256]{2,1,0:T(8,128)(2,1)}), bf16[8,48,256]{2,1,0:T(8,128)(2,1)S(1)}, u32[]{:S(2)}, u32[]{:S(2)}) async-start(bf16[8,48,256]{2,1,0:T(8,128)(2,1)} %broadcast_in_dim.13), calls=%async_computation.3 | async-start | bytes 393216 | tf_op jit(solution)/shard_map/all_to_all | solution.py:105
  92.4 0.8 dynamic_slice.20
  93.2 0.1 fusion.5
  93.3 0.1 pad_maximum_fusion
  93.4 0.1 copy.76
  93.4 9.9 %all-to-all-done.3 = bf16[8,48,256]{2,1,0:T(8,128)(2,1)S(1)} async-done(((bf16[8,48,256]{2,1,0:T(8,128)(2,1)}), bf16[8,48,256]{2,1,0:T(8,128)(2,1)S(1)}, u32[]{:S(2)}, u32[]{:S(2)}) %all-to-all-start.3) | async-done | bytes 196640 | tf_op jit(solution)/shard_map/all_to_all | solution.py:105
  103.4 0.1 broadcast_in_dim.12
  103.5 57.5 %all_to_all.54 = bf16[64,2,16,256]{3,2,1,0:T(8,128)(2,1)S(1)} all-to-all(bf16[64,2,16,256]{3,2,1,0:T(8,128)(2,1)S(1)} %bitcast.70), channel_id=1, replica_groups=mesh['gr'=2,'zl'=8,'y'=4,'x'=4,'core'=2] {'gr','zl','y'}, dimensions={0} | all-to-all | bytes 2097152 | tf_op jit(solution)/shard_map/all_to_all | solution.py:147
  161.0 1.0 broadcast_in_dim.14
  161.9 7.9 %all-to-all-start.4 = ((bf16[4,8,48,256]{3,2,1,0:T(8,128)(2,1)}), bf16[4,8,48,256]{3,2,1,0:T(8,128)(2,1)S(1)}, u32[]{:S(2)}, u32[]{:S(2)}) async-start(bf16[4,8,48,256]{3,2,1,0:T(8,128)(2,1)} %broadcast_in_dim.14), calls=%async_computation.4 | async-start | bytes 1572864 | tf_op jit(solution)/shard_map/all_to_all | solution.py:105
  169.9 1.1 copy.77
  171.0 7.3 %all-to-all-done.4 = bf16[4,8,48,256]{3,2,1,0:T(8,128)(2,1)S(1)} async-done(((bf16[4,8,48,256]{3,2,1,0:T(8,128)(2,1)}), bf16[4,8,48,256]{3,2,1,0:T(8,128)(2,1)S(1)}, u32[]{:S(2)}, u32[]{:S(2)}) %all-to-all-start.4) | async-done | bytes 786464 | tf_op jit(solution)/shard_map/all_to_all | solution.py:105
  178.2 9.9 %all-to-all-start.2 = ((bf16[8,2,2,4,16,256]{5,4,1,3,2,0:T(8,128)(2,1)}), bf16[8,2,2,4,16,256]{5,4,1,3,2,0:T(8,128)(2,1)S(1)}, u32[]{:S(2)}, u32[]{:S(2)}) async-start(bf16[8,2,2,4,16,256]{5,4,1,3,2,0:T(8,128)(2,1)} %copy.77), calls=%async_computation.2 | async-start | bytes 2097152 | tf_op jit(solution)/shard_map/all_to_all | solution.py:155
  188.1 1.0 copy.94
  189.1 1.1 slice.78
  190.2 0.1 reshape.112
  190.3 0.1 copy.82
  190.4 0.4 fusion.20
  190.9 12.2 %all-to-all-done.2 = bf16[8,2,2,4,16,256]{5,4,1,3,2,0:T(8,128)(2,1)S(1)} async-done(((bf16[8,2,2,4,16,256]{5,4,1,3,2,0:T(8,128)(2,1)}), bf16[8,2,2,4,16,256]{5,4,1,3,2,0:T(8,128)(2,1)S(1)}, u32[]{:S(2)}, u32[]{:S(2)}) %all-to-all-start.2) | async-done | bytes 1048608 | tf_op jit(solution)/shard_map/all_to_all | solution.py:155
  203.1 0.1 copy.78
  203.2 0.1 fusion.17
  203.4 0.3 copy.79
  203.7 0.2 reshape_squeeze.6.gate_ref
  203.9 0.5 copy-done.1
  204.4 0.3 copy.80
  204.8 0.2 reshape_squeeze.7.up_ref
  205.0 0.0 all-gather.2.cloned.1.call-done
  205.0 7.5 %gate_up.1 = bf16[64,2304]{1,0:T(8,128)(2,1)S(1)} custom-call(bf16[8,2304,256]{2,1,0:T(8,128)(2,1)} %bitcast.62, bf16[2,64,2048]{2,1,0:T(8,128)(2,1)S(1)} %reshape_squeeze.6.gate_ref, bf16[2,64,2048]{2,1,0:T(8,128)(2,1)S(1)} %reshape_squeeze.7.up_ref), custom_call_target="tpu_custom_call" | custom-call | flops 2415919104 | bytes 9437184 | tf_op jit(solution)/shard_map/gate_up/pallas_call | solution.py:179
  212.5 1.2 broadcast_in_dim.15
  213.7 3.7 %all-to-all-start.5 = ((bf16[4,64,2496]{2,1,0:T(8,128)(2,1)}), bf16[4,64,2496]{2,1,0:T(8,128)(2,1)S(1)}, u32[]{:S(2)}, u32[]{:S(2)}) async-start(bf16[4,64,2496]{2,1,0:T(8,128)(2,1)} %broadcast_in_dim.15), calls=%async_computation.5 | async-start | bytes 2621440 | tf_op jit(solution)/shard_map/all_to_all | solution.py:105
  217.4 16.9 %all-to-all-done.5 = bf16[4,64,2496]{2,1,0:T(8,128)(2,1)S(1)} async-done(((bf16[4,64,2496]{2,1,0:T(8,128)(2,1)}), bf16[4,64,2496]{2,1,0:T(8,128)(2,1)S(1)}, u32[]{:S(2)}, u32[]{:S(2)}) %all-to-all-start.5) | async-done | bytes 1277984 | tf_op jit(solution)/shard_map/all_to_all | solution.py:105
  234.4 0.8 broadcast_in_dim.17
  235.2 4.6 %all-to-all-start.6 = ((bf16[64,16,256]{2,1,0:T(8,128)(2,1)}), bf16[64,16,256]{2,1,0:T(8,128)(2,1)S(1)}, u32[]{:S(2)}, u32[]{:S(2)}) async-start(bf16[64,16,256]{2,1,0:T(8,128)(2,1)} %bitcast.17), calls=%async_computation.6 | async-start | bytes 1048576 | tf_op jit(solution)/shard_map/all_to_all | solution.py:150
  239.9 1.5 copy.85
  241.4 3.8 %collective-permute-start = (bf16[256,2496]{0,1:T(8,128)(2,1)}, bf16[256,2496]{0,1:T(8,128)(2,1)}, u32[]{:S(2)}, u32[]{:S(2)}) collective-permute-start(bf16[256,2496]{0,1:T(8,128)(2,1)} %copy.85), channel_id=1, source_target_pairs={{0,1},{1,0},{2,3},{3,2},{4,5},{5,4},{6,7},{7,6},{8,9},{9,8},{10,11... | collective-permute-start | bytes 3833864 | tf_op jit(solution)/shard_map/ppermute | solution.py:197
  245.2 23.7 %all-to-all-done.6 = bf16[64,16,256]{2,1,0:T(8,128)(2,1)S(1)} async-done(((bf16[64,16,256]{2,1,0:T(8,128)(2,1)}), bf16[64,16,256]{2,1,0:T(8,128)(2,1)S(1)}, u32[]{:S(2)}, u32[]{:S(2)}) %all-to-all-start.6) | async-done | bytes 524320 | tf_op jit(solution)/shard_map/all_to_all | solution.py:150
  268.9 0.8 fusion.2
  269.8 2.0 convolution_add_fusion
  271.8 2.8 fusion
  274.6 8.4 %all-to-all-start.7 = ((bf16[32,72,256]{2,1,0:T(8,128)(2,1)}), bf16[32,72,256]{2,1,0:T(8,128)(2,1)S(1)}, u32[]{:S(2)}, u32[]{:S(2)}) async-start(bf16[32,72,256]{2,1,0:T(8,128)(2,1)} %bitcast.65), calls=%async_computation.7 | async-start | bytes 2359296 | tf_op jit(solution)/shard_map/all_to_all | solution.py:214
  283.1 1.7 slice.88
  284.8 1.1 fusion.18
  285.9 2.0 copy.90
  287.9 1.9 copy.91
  289.8 1.0 constant_dynamic-slice_fusion
  290.8 1.0 broadcast_in_dim_reshape_squeeze.6
  291.9 2.1 broadcast_in_dim_reshape_squeeze.7
  293.9 0.2 fusion.8
  294.1 1.1 convolution_add_fusion.1.shared_ref
  295.2 43.0 %all-to-all-done.7 = bf16[32,72,256]{2,1,0:T(8,128)(2,1)S(1)} async-done(((bf16[32,72,256]{2,1,0:T(8,128)(2,1)}), bf16[32,72,256]{2,1,0:T(8,128)(2,1)S(1)}, u32[]{:S(2)}, u32[]{:S(2)}) %all-to-all-start.7) | async-done | bytes 1179680 | tf_op jit(solution)/shard_map/all_to_all | solution.py:214
  338.2 2.4 mix.1
  340.7 0.8 copy.96
  (31 shorter events, 0.3 us)
Async XLA Ops:
  7.2 197.9 %all-gather.2.cloned.1.call-start = ((), (), s32[]{:S(2)}) async-start(), calls=%async_computation.8 | async-start | bytes 10616832 | tf_op jit(solution)/shard_map/all_gather | solution.py:140
  8.8 1.1 copy-start
  11.6 73.8 %copy-start.11 = (f32[16,256]{1,0:T(8,128)S(1)}, f32[16,256]{1,0:T(8,128)}, u32[]{:S(2)}) copy-start(f32[16,256]{1,0:T(8,128)} %param.19) | copy-start | bytes 49156
  11.6 74.6 %copy-start.9 = (f32[64,64]{1,0:T(8,128)S(1)}, f32[64,64]{1,0:T(8,128)}, u32[]{:S(2)}) copy-start(f32[64,64]{1,0:T(8,128)} %param.17) | copy-start | bytes 49156
  11.6 74.6 %copy-start.10 = (f32[64,64]{1,0:T(8,128)S(1)}, f32[64,64]{1,0:T(8,128)}, u32[]{:S(2)}) copy-start(f32[64,64]{1,0:T(8,128)} %param.18) | copy-start | bytes 49156
  85.4 7.8 %copy-start.7 = (f32[1,32,16,256]{3,2,1,0:T(8,128)S(1)}, f32[1,32,16,256]{3,2,1,0:T(8,128)}, u32[]{:S(2)}) copy-start(f32[1,32,16,256]{3,2,1,0:T(8,128)} %param.14) | copy-start | bytes 1572868
  85.4 7.8 %copy-start.8 = (f32[1,32,16,256]{3,2,1,0:T(8,128)S(1)}, f32[1,32,16,256]{3,2,1,0:T(8,128)}, u32[]{:S(2)}) copy-start(f32[1,32,16,256]{3,2,1,0:T(8,128)} %param.15) | copy-start | bytes 1572868
  87.2 16.2 %all-to-all-start.3 = ((bf16[8,48,256]{2,1,0:T(8,128)(2,1)}), bf16[8,48,256]{2,1,0:T(8,128)(2,1)S(1)}, u32[]{:S(2)}, u32[]{:S(2)}) async-start(bf16[8,48,256]{2,1,0:T(8,128)(2,1)} %broadcast_in_dim.13), calls=%async_computation.3 | async-start | bytes 393216 | tf_op jit(solution)/shard_map/all_to_all | solution.py:105
  161.9 16.3 %all-to-all-start.4 = ((bf16[4,8,48,256]{3,2,1,0:T(8,128)(2,1)}), bf16[4,8,48,256]{3,2,1,0:T(8,128)(2,1)S(1)}, u32[]{:S(2)}, u32[]{:S(2)}) async-start(bf16[4,8,48,256]{3,2,1,0:T(8,128)(2,1)} %broadcast_in_dim.14), calls=%async_computation.4 | async-start | bytes 1572864 | tf_op jit(solution)/shard_map/all_to_all | solution.py:105
  178.2 24.9 %all-to-all-start.2 = ((bf16[8,2,2,4,16,256]{5,4,1,3,2,0:T(8,128)(2,1)}), bf16[8,2,2,4,16,256]{5,4,1,3,2,0:T(8,128)(2,1)S(1)}, u32[]{:S(2)}, u32[]{:S(2)}) async-start(bf16[8,2,2,4,16,256]{5,4,1,3,2,0:T(8,128)(2,1)} %copy.77), calls=%async_computation.2 | async-start | bytes 2097152 | tf_op jit(solution)/shard_map/all_to_all | solution.py:155
  203.7 0.8 copy-start.1
  204.7 7.8 %copy-start.3 = (bf16[1,2,64,8,256]{4,3,2,1,0:T(8,128)(2,1)}, bf16[1,2,64,8,256]{4,3,2,1,0:T(8,128)(2,1)S(1)}, u32[]{:S(2)}) copy-start(bf16[1,2,64,8,256]{4,3,2,1,0:T(8,128)(2,1)S(1)} %copy.80) | copy-start | bytes 1572868
  213.7 3.7 %copy-start.6 = (f32[1,32,16,256]{3,2,1,0:T(8,128)S(1)}, f32[1,32,16,256]{3,2,1,0:T(8,128)}, u32[]{:S(2)}) copy-start(f32[1,32,16,256]{3,2,1,0:T(8,128)} %param.16) | copy-start | bytes 1572868
  213.7 20.7 %all-to-all-start.5 = ((bf16[4,64,2496]{2,1,0:T(8,128)(2,1)}), bf16[4,64,2496]{2,1,0:T(8,128)(2,1)S(1)}, u32[]{:S(2)}, u32[]{:S(2)}) async-start(bf16[4,64,2496]{2,1,0:T(8,128)(2,1)} %broadcast_in_dim.15), calls=%async_computation.5 | async-start | bytes 2621440 | tf_op jit(solution)/shard_map/all_to_all | solution.py:105
  235.2 33.6 %all-to-all-start.6 = ((bf16[64,16,256]{2,1,0:T(8,128)(2,1)}), bf16[64,16,256]{2,1,0:T(8,128)(2,1)S(1)}, u32[]{:S(2)}, u32[]{:S(2)}) async-start(bf16[64,16,256]{2,1,0:T(8,128)(2,1)} %bitcast.17), calls=%async_computation.6 | async-start | bytes 1048576 | tf_op jit(solution)/shard_map/all_to_all | solution.py:150
  241.4 28.4 %collective-permute-start = (bf16[256,2496]{0,1:T(8,128)(2,1)}, bf16[256,2496]{0,1:T(8,128)(2,1)}, u32[]{:S(2)}, u32[]{:S(2)}) collective-permute-start(bf16[256,2496]{0,1:T(8,128)(2,1)} %copy.85), channel_id=1, source_target_pairs={{0,1},{1,0},{2,3},{3,2},{4,5},{5,4},{6,7},{7,6},{8,9},{9,8},{10,11... | collective-permute-start | bytes 3833864 | tf_op jit(solution)/shard_map/ppermute | solution.py:197
  268.9 0.9 copy-start.4
  274.6 63.6 %all-to-all-start.7 = ((bf16[32,72,256]{2,1,0:T(8,128)(2,1)}), bf16[32,72,256]{2,1,0:T(8,128)(2,1)S(1)}, u32[]{:S(2)}, u32[]{:S(2)}) async-start(bf16[32,72,256]{2,1,0:T(8,128)(2,1)} %bitcast.65), calls=%async_computation.7 | async-start | bytes 2359296 | tf_op jit(solution)/shard_map/all_to_all | solution.py:214
  285.9 4.9 %copy-start.2 = (bf16[1,2,64,8,256]{4,3,2,1,0:T(8,128)(2,1)S(1)}, bf16[1,2,64,8,256]{4,3,2,1,0:T(8,128)(2,1)}, u32[]{:S(2)}) copy-start(bf16[1,2,64,8,256]{4,3,2,1,0:T(8,128)(2,1)} %copy-done.1) | copy-start | bytes 1572868
  293.9 46.7 %copy-start.5 = (bf16[64,16,256]{2,1,0:T(8,128)(2,1)S(1)}, bf16[64,16,256]{2,1,0:T(8,128)(2,1)}, u32[]{:S(2)}) copy-start(bf16[64,16,256]{2,1,0:T(8,128)(2,1)} %copy-done.4) | copy-start | bytes 1572868
Sparse Core Ops, SparseCore 0:
  85.5 58.5 all-gather.1
